TPU v7x, 32 devices: a whole 2x2x4 slice. The times are simulated.
32 devices in a mesh: rep: 4 (over z), fs: 2 (over y), tp: 4 (over x, core).
Axes of the slice: x: 2, y: 2, z: 4, core: 2. Of those that a mesh axis runs over, the one named last changes fastest.
Arguments:
- inputs: bfloat16 [512, 4096], P('rep'), may hold values from -6 to 6
- cotangent: bfloat16 [512, 4096], P('rep'), may hold values from -6 to 6
- w_gate: bfloat16 [4096, 11264], P(None, ('fs', 'tp')), may hold values from -0.09375 to 0.09375
- w_upward: bfloat16 [4096, 11264], P(None, ('fs', 'tp')), may hold values from -0.09375 to 0.09375
- w_down: bfloat16 [11264, 4096], P(('fs', 'tp')), may hold values from -0.0546875 to 0.0546875
Outputs:
- grad_input: bfloat16 [512, 4096], P('rep')
- grad_gate: float32 [4096, 11264], P('rep', ('fs', 'tp'))
- grad_upward: float32 [4096, 11264], P('rep', ('fs', 'tp'))
- grad_down: float32 [11264, 4096], P(('fs', 'tp'), 'rep')
All inputs are finite; a program needn't handle non-finite values.
Results may differ from a plain program's by a relative error of at most 0.0049.
Values may be sent and summed in bfloat16 or wider, within the bound.
A program may use at most 128 MiB of HBM per device.

v0:
```python
import jax
import jax.numpy as jnp
from jax import lax
from jax.sharding import PartitionSpec as P


def contract_rows(left, right):
    return lax.dot_general(
        left, right, (((0,), (0,)), ((), ())), preferred_element_type=jnp.float32
    )


def contract_cols(left, right):
    return lax.dot_general(
        left, right, (((1,), (1,)), ((), ())), preferred_element_type=jnp.float32
    )


def local(inputs, cotangent, w_gate, w_upward, w_down):
    gate_pre = jnp.dot(inputs, w_gate, preferred_element_type=jnp.float32)
    up_pre = jnp.dot(inputs, w_upward, preferred_element_type=jnp.float32)
    sigmoid_gate = jax.nn.sigmoid(gate_pre)
    activated = gate_pre * sigmoid_gate
    hidden = (activated * up_pre).astype(jnp.bfloat16)
    hidden_grad = contract_cols(cotangent, w_down)
    gate_delta = (
        hidden_grad * up_pre * sigmoid_gate * (1.0 + gate_pre * (1.0 - sigmoid_gate))
    ).astype(jnp.bfloat16)
    up_delta = (hidden_grad * activated).astype(jnp.bfloat16)
    input_cols, cotangent_cols = (
        lax.all_to_all(inputs, "rep", split_axis=1, concat_axis=0, tiled=True),
        lax.all_to_all(cotangent, "rep", split_axis=1, concat_axis=0, tiled=True),
    )
    piece_gate = lax.all_gather(gate_delta, "rep", axis=0, tiled=True)
    piece_up = lax.all_gather(up_delta, "rep", axis=0, tiled=True)
    piece_hidden = lax.all_gather(hidden, "rep", axis=0, tiled=True)
    grad_gate = contract_rows(input_cols, piece_gate)
    grad_upward = contract_rows(input_cols, piece_up)
    grad_down = contract_rows(piece_hidden, cotangent_cols)
    input_terms = contract_cols(gate_delta, w_gate) + contract_cols(up_delta, w_upward)
    grad_input = lax.psum(input_terms, ("fs", "tp")).astype(jnp.bfloat16)
    return (grad_input, grad_gate, grad_upward, grad_down)


def solution(mesh):
    in_specs = (
        P("rep", None),
        P("rep", None),
        P(None, ("fs", "tp")),
        P(None, ("fs", "tp")),
        P(("fs", "tp"), None),
    )
    out_specs = (
        P("rep", None),
        P("rep", ("fs", "tp")),
        P("rep", ("fs", "tp")),
        P(("fs", "tp"), "rep"),
    )
    return jax.shard_map(local, mesh=mesh, in_specs=in_specs, out_specs=out_specs, check_vma=False)
```

profile of v0, /device:TPU:0, one launch (start us, length us, event | category | flops | bytes accessed | tf_op | source)
XLA Modules:
  0.0 190.2 jit_solution(5874101361756558968)
XLA Ops:
  7.2 0.0 copy-start.2
  7.2 0.0 all-gather.4.cloned.1.call-start
  7.2 0.0 copy-start
  7.2 8.6 %fusion.1 = f32[128,1408]{1,0:T(8,128)S(1)} fusion(bf16[128,4096]{1,0:T(8,128)(2,1)} %param.6, bf16[1408,4096]{1,0:T(8,128)(2,1)} %param.9), kind=kOutput, calls=%fused_computation.8 | convolution fusion | flops 1476395008 | bytes 13303808 | tf_op jit(solution)/shard_map/dot_general | solution.py:14
  15.8 0.0 copy-done.2
  15.8 0.0 copy-done
  15.8 0.0 copy-start.1
  15.8 1.8 fusion.2
  17.7 2.4 %copy-done.1 = bf16[4096,1408]{1,0:T(8,128)(2,1)S(1)} copy-done((bf16[4096,1408]{1,0:T(8,128)(2,1)S(1)}, bf16[4096,1408]{1,0:T(8,128)(2,1)}, u32[]{:S(2)}) %copy-start.1) | copy-done | bytes 11534360
  20.1 3.0 %multiply_convert_fusion = (bf16[128,1408]{1,0:T(8,128)(2,1)}, bf16[128,1408]{1,0:T(8,128)(2,1)}, bf16[128,1408]{1,0:T(8,128)(2,1)}) fusion(f32[128,1408]{1,0:T(8,128)S(1)} %fusion.2, f32[128,1408]{1,0:T(8,128)S(1)} %fusion.1, bf16[128,4096]{1,0:T(8,128)(2,1)S(1)} %copy-done.2, bf16[4096,1408]{1,0:T(8,128)(2,1)S(1)} %copy-done.1), kind=kOutput, calls=%fused_computation.3 | convolution fusion | flops 1479098368 | bytes 15106048 | tf_op jit(solution)/shard_map/dot_general | solution.py:21
  23.1 0.0 all-gather.4.cloned.1.call-update
  23.1 0.0 all-gather.6.cloned.1.call-start
  23.2 0.7 all-gather.6.cloned.1.call-update
  23.9 1.3 copy.13
  25.2 6.3 %all-to-all-start = ((bf16[128,4,1024]{0,2,1:T(8,128)(2,1)}), bf16[128,4,1024]{0,2,1:T(8,128)(2,1)S(1)}, u32[]{:S(2)}, u32[]{:S(2)}) async-start(bf16[128,4,1024]{0,2,1:T(8,128)(2,1)} %bitcast.27), calls=%async_computation | async-start | bytes 2097152 | tf_op jit(solution)/shard_map/all_to_all | solution.py:31
  31.5 0.7 all-gather.8.cloned.1.call-update
  32.3 0.0 copy-done.3
  32.3 1.3 copy.15
  33.6 9.5 %fusion.3 = f32[128,4096]{1,0:T(8,128)} fusion(bf16[128,1408]{1,0:T(8,128)(2,1)S(1)} %copy-done.4, bf16[4096,1408]{1,0:T(8,128)(2,1)} %param.7), kind=kOutput, calls=%fused_computation.10 | convolution fusion | flops 1476395008 | bytes 13991936 | tf_op jit(solution)/shard_map/dot_general | solution.py:14
  43.1 37.0 %all-to-all-done = bf16[128,4,1024]{0,2,1:T(8,128)(2,1)S(1)} async-done(((bf16[128,4,1024]{0,2,1:T(8,128)(2,1)}), bf16[128,4,1024]{0,2,1:T(8,128)(2,1)S(1)}, u32[]{:S(2)}, u32[]{:S(2)}) %all-to-all-start) | async-done | bytes 1048608 | tf_op jit(solution)/shard_map/all_to_all | solution.py:31
  80.1 4.3 %all-to-all-start.1 = ((bf16[128,4,1024]{0,2,1:T(8,128)(2,1)}), bf16[128,4,1024]{0,2,1:T(8,128)(2,1)}, u32[]{:S(2)}, u32[]{:S(2)}) async-start(bf16[128,4,1024]{0,2,1:T(8,128)(2,1)} %bitcast.5), calls=%async_computation.1 | async-start | bytes 2097152 | tf_op jit(solution)/shard_map/all_to_all | solution.py:32
  84.3 9.0 %convolution_add_fusion = f32[128,4096]{1,0:T(8,128)S(1)} fusion(f32[128,4096]{1,0:T(8,128)} %fusion.3, bf16[128,1408]{1,0:T(8,128)(2,1)} %get-tuple-element.18, bf16[4096,1408]{1,0:T(8,128)(2,1)} %param.8), kind=kOutput, calls=%fused_computation | convolution fusion | flops 1476919296 | bytes 16089088 | tf_op jit(solution)/shard_map/dot_general | solution.py:14
  93.3 59.1 %all-reduce.1 = bf16[128,4096]{1,0:T(8,128)(2,1)} all-reduce(f32[128,4096]{1,0:T(8,128)S(1)} %convolution_add_fusion), channel_id=1, replica_groups=mesh['rep'=4,'fs'=2,'tp'=4] {'fs','tp'}, use_global_device_ids=true, to_apply=%region_0.0 | all-reduce | flops 524288 | bytes 3145728 | tf_op jit(solution)/shard_map/psum | solution.py:41
  152.4 0.5 copy.14
  153.0 0.0 all-to-all-done.1
  153.0 1.5 copy.16
  154.5 0.0 all-gather.4.cloned.1.call-done
  154.5 5.6 %convolution_bitcast_fusion.1 = f32[1024,1408]{0,1:T(8,128)} fusion(bf16[512,1408]{1,0:T(8,128)(2,1)} %all-gather.4.cloned.1.call-done, bf16[512,1024]{1,0:T(8,128)(2,1)S(1)} %bitcast.29), kind=kOutput, calls=%fused_computation.2 | convolution fusion | flops 1476395008 | bytes 8257536 | tf_op jit(solution)/shard_map/dot_general | solution.py:8
  160.1 6.2 %copy.17 = f32[1024,1408]{1,0:T(8,128)} copy(f32[1024,1408]{0,1:T(8,128)} %convolution_bitcast_fusion.1) | data formatting | bytes 11534336
  166.3 5.6 %convolution_bitcast_fusion = f32[1024,1408]{0,1:T(8,128)} fusion(bf16[512,1408]{1,0:T(8,128)(2,1)} %all-gather.6.cloned.1.call-done, bf16[512,1024]{1,0:T(8,128)(2,1)S(1)} %bitcast.30), kind=kOutput, calls=%fused_computation.1 | convolution fusion | flops 1476395008 | bytes 8257536 | tf_op jit(solution)/shard_map/dot_general | solution.py:8
  171.9 6.2 %copy.18 = f32[1024,1408]{1,0:T(8,128)} copy(f32[1024,1408]{0,1:T(8,128)} %convolution_bitcast_fusion) | data formatting | bytes 11534336
  178.1 5.6 %fusion.4 = f32[1408,1024]{1,0:T(8,128)} fusion(bf16[512,1408]{1,0:T(8,128)(2,1)} %all-gather.8.cloned.1.call-done, bf16[512,1024]{1,0:T(8,128)(2,1)S(1)} %bitcast.28), kind=kOutput, calls=%fused_computation.11 | convolution fusion | flops 1476395008 | bytes 8257536 | tf_op jit(solution)/shard_map/dot_general | solution.py:8
  (6 shorter events, 0.0 us)
Async XLA Ops:
  7.2 8.6 %copy-start.2 = (bf16[128,4096]{1,0:T(8,128)(2,1)S(1)}, bf16[128,4096]{1,0:T(8,128)(2,1)}, u32[]{:S(2)}) copy-start(bf16[128,4096]{1,0:T(8,128)(2,1)} %param.5) | copy-start | bytes 3145732
  7.2 147.3 %all-gather.4.cloned.1.call-start = ((), (), s32[]{:S(2)}) async-start(), calls=%async_computation.2 | async-start | bytes 1802240 | tf_op jit(solution)/shard_map/all_gather | solution.py:34
  7.2 8.6 %copy-start = (bf16[4096,1408]{1,0:T(8,128)(2,1)S(1)}, bf16[4096,1408]{1,0:T(8,128)(2,1)}, u32[]{:S(2)}) copy-start(bf16[4096,1408]{1,0:T(8,128)(2,1)} %param.7) | copy-start | bytes 34603012
  15.8 4.3 %copy-start.1 = (bf16[4096,1408]{1,0:T(8,128)(2,1)S(1)}, bf16[4096,1408]{1,0:T(8,128)(2,1)}, u32[]{:S(2)}) copy-start(bf16[4096,1408]{1,0:T(8,128)(2,1)} %param.8) | copy-start | bytes 34603012
  23.1 9.2 %copy-start.3 = (bf16[128,4096]{1,0:T(8,128)(2,1)S(1)}, bf16[128,4096]{1,0:T(8,128)(2,1)}, u32[]{:S(2)}) copy-start(bf16[128,4096]{1,0:T(8,128)(2,1)} %param.6) | copy-start | bytes 3145732
  23.1 10.5 %copy-start.4 = (bf16[128,1408]{1,0:T(8,128)(2,1)S(1)}, bf16[128,1408]{1,0:T(8,128)(2,1)}, u32[]{:S(2)}) copy-start(bf16[128,1408]{1,0:T(8,128)(2,1)} %get-tuple-element.17) | copy-start | bytes 1081348
  23.1 143.2 %all-gather.6.cloned.1.call-start = ((), (), s32[]{:S(2)}) async-start(), calls=%async_computation.3 | async-start | bytes 1802240 | tf_op jit(solution)/shard_map/all_gather | solution.py:35
  25.2 54.9 %all-to-all-start = ((bf16[128,4,1024]{0,2,1:T(8,128)(2,1)}), bf16[128,4,1024]{0,2,1:T(8,128)(2,1)S(1)}, u32[]{:S(2)}, u32[]{:S(2)}) async-start(bf16[128,4,1024]{0,2,1:T(8,128)(2,1)} %bitcast.27), calls=%async_computation | async-start | bytes 2097152 | tf_op jit(solution)/shard_map/all_to_all | solution.py:31
  31.5 146.6 %all-gather.8.cloned.1.call-start = ((), (), s32[]{:S(2)}) async-start(), calls=%async_computation.4 | async-start | bytes 1802240 | tf_op jit(solution)/shard_map/all_gather | solution.py:36
  80.1 72.9 %all-to-all-start.1 = ((bf16[128,4,1024]{0,2,1:T(8,128)(2,1)}), bf16[128,4,1024]{0,2,1:T(8,128)(2,1)}, u32[]{:S(2)}, u32[]{:S(2)}) async-start(bf16[128,4,1024]{0,2,1:T(8,128)(2,1)} %bitcast.5), calls=%async_computation.1 | async-start | bytes 2097152 | tf_op jit(solution)/shard_map/all_to_all | solution.py:32
Sparse Core Ops, SparseCore 0:
  23.2 57.4 all-gather.3
  82.3 48.3 all-gather.5
  132.3 33.8 all-gather.7
where the time goes:
time: 191 us; the launch traced here: 190 us
  blocking collectives  59.1 us (31%)
  matrix products  48.6 us (25%)
  waiting for transfers between devices  38.5 us (20%)
  local copies, waits for them, and re-layouts  19.5 us (10%)
  between operations  13.9 us (7%)
  starting transfers between devices  10.7 us (6%)
    psum x1, blocking collectives, local(): grad_input = lax.psum(input_terms, ('fs', 'tp')).astype(jnp.bfloat16)  59.1 us
    all_to_all x1, waiting for transfers between devices, local(): lax.all_to_all(inputs, 'rep', split_axis=1, concat_axis=0, tiled=True)  37 us
    dot_general x3, matrix products, contract_cols(): lax.dot_general(left, right, (((1,), (1,)), ((), ())), preferred_element_...  27 us
    unnamed x14, local copies, waits for them, and re-layouts  17.5 us
    dot_general x3, matrix products, contract_rows(): lax.dot_general(left, right, (((0,), (0,)), ((), ())), preferred_element_...  16.7 us
    all_to_all x1, starting transfers between devices, local(): lax.all_to_all(inputs, 'rep', split_axis=1, concat_axis=0, tiled=True)  6.35 us
    all_to_all x1, starting transfers between devices, local(): lax.all_to_all(cotangent, 'rep', split_axis=1, concat_axis=0, tiled=True)  4.27 us
  transfers between devices with their start and end apart: 5, of which 1 were waited for; matrix products, arithmetic and copies ran while one was open for 25% of the time, Pallas kernels for 0%

commit v1 on v0

--- a/solution.py
+++ b/solution.py
@@ -38,7 +38,7 @@
     grad_upward = contract_rows(input_cols, piece_up)
     grad_down = contract_rows(piece_hidden, cotangent_cols)
     input_terms = contract_cols(gate_delta, w_gate) + contract_cols(up_delta, w_upward)
-    grad_input = lax.psum(input_terms, ("fs", "tp")).astype(jnp.bfloat16)
+    grad_input = lax.psum(lax.psum(input_terms, "fs"), "tp").astype(jnp.bfloat16)
     return (grad_input, grad_gate, grad_upward, grad_down)
 
 

time: 191 us -> 225 us (1.18)
  waiting for transfers between devices: 38.5 us -> 90.6 us
  blocking collectives: 59.1 us -> 41.5 us
    all_to_all x1, waiting for transfers between devices: 0.01 us -> 42.2 us  [local(): lax.all_to_all(cotangent, 'rep', split_axis=1, concat_axis=0, tiled=True)]
    psum x1, blocking collectives: 59.1 us -> 41.5 us  [local(): lax.psum(lax.psum(input_terms, 'fs'), 'tp').astype(jnp.bfloat16)]
    all_to_all x1, waiting for transfers between devices: 37 us -> 46.7 us  [local(): lax.all_to_all(inputs, 'rep', split_axis=1, concat_axis=0, tiled=True)]
  transfers between devices with their start and end apart: 5 -> 6, of which waited for: 1 -> 2; matrix products, arithmetic and copies ran while one was open for 25% -> 12% of each run, Pallas kernels for 0% -> 0%
where the time goes in v1:
time: 225 us; the launch traced here: 224 us
  waiting for transfers between devices  90.6 us (40%)
  matrix products  47.7 us (21%)
  blocking collectives  41.5 us (18%)
  local copies, waits for them, and re-layouts  18.6 us (8%)
  between operations  15.8 us (7%)
  starting transfers between devices  9.98 us (4%)
    all_to_all x1, waiting for transfers between devices, local(): lax.all_to_all(inputs, 'rep', split_axis=1, concat_axis=0, tiled=True)  46.7 us
    all_to_all x1, waiting for transfers between devices, local(): lax.all_to_all(cotangent, 'rep', split_axis=1, concat_axis=0, tiled=True)  42.2 us
    psum x1, blocking collectives, local(): lax.psum(lax.psum(input_terms, 'fs'), 'tp').astype(jnp.bfloat16)  41.5 us
    dot_general x3, matrix products, contract_cols(): lax.dot_general(left, right, (((1,), (1,)), ((), ())), preferred_element_...  26.3 us
    unnamed x14, local copies, waits for them, and re-layouts  17.5 us
    dot_general x3, matrix products, contract_rows(): lax.dot_general(left, right, (((0,), (0,)), ((), ())), preferred_element_...  16.7 us
    all_to_all x1, starting transfers between devices, local(): lax.all_to_all(inputs, 'rep', split_axis=1, concat_axis=0, tiled=True)  6.34 us
  transfers between devices with their start and end apart: 6, of which 2 were waited for; matrix products, arithmetic and copies ran while one was open for 12% of the time, Pallas kernels for 0%

profile of v1, /device:TPU:0, one launch (start us, length us, event | category | flops | bytes accessed | tf_op | source)
XLA Modules:
  0.0 224.1 jit_solution(6366149549941727887)
XLA Ops:
  8.0 0.0 all-reduce.3.cloned.1.call-start
  8.1 0.0 copy-start
  8.1 8.6 %fusion.1 = f32[128,1408]{1,0:T(8,128)S(1)} fusion(bf16[128,4096]{1,0:T(8,128)(2,1)} %param.6, bf16[1408,4096]{1,0:T(8,128)(2,1)} %param.9), kind=kOutput, calls=%fused_computation.8 | convolution fusion | flops 1476395008 | bytes 13303808 | tf_op jit(solution)/shard_map/dot_general | solution.py:14
  16.7 0.0 copy-start.1
  16.7 1.8 fusion.2
  18.5 2.4 %copy-done.1 = bf16[4096,1408]{1,0:T(8,128)(2,1)S(1)} copy-done((bf16[4096,1408]{1,0:T(8,128)(2,1)S(1)}, bf16[4096,1408]{1,0:T(8,128)(2,1)}, u32[]{:S(2)}) %copy-start.1) | copy-done | bytes 11534360
  20.9 2.9 %multiply_convert_fusion = (bf16[128,1408]{1,0:T(8,128)(2,1)}, bf16[128,1408]{1,0:T(8,128)(2,1)S(1)}, bf16[128,1408]{1,0:T(8,128)(2,1)}) fusion(f32[128,1408]{1,0:T(8,128)S(1)} %fusion.2, f32[128,1408]{1,0:T(8,128)S(1)} %fusion.1, bf16[128,4096]{1,0:T(8,128)(2,1)S(1)} %copy-done.2, bf16[4096,1408]{1,0:T(8,128)(2,1)S(1)} %copy-done.1), kind=kOutput, calls=%fused_computation.3 | convolution fusion | flops 1479098368 | bytes 15106048 | tf_op jit(solution)/shard_map/dot_general | solution.py:21
  23.8 8.2 %fusion.3 = f32[128,4096]{1,0:T(8,128)S(1)} fusion(bf16[128,1408]{1,0:T(8,128)(2,1)S(1)} %get-tuple-element.17, bf16[4096,1408]{1,0:T(8,128)(2,1)} %param.7), kind=kOutput, calls=%fused_computation.10 | convolution fusion | flops 1476395008 | bytes 13991936 | tf_op jit(solution)/shard_map/dot_general | solution.py:14
  32.0 0.0 copy-done.4
  32.0 9.5 %convolution_add_fusion = f32[128,4096]{1,0:T(8,128)} fusion(f32[128,4096]{1,0:T(8,128)S(1)} %fusion.3, bf16[128,1408]{1,0:T(8,128)(2,1)} %get-tuple-element.18, bf16[4096,1408]{1,0:T(8,128)(2,1)} %param.8), kind=kOutput, calls=%fused_computation | convolution fusion | flops 1476919296 | bytes 16089088 | tf_op jit(solution)/shard_map/dot_general | solution.py:14
  41.5 0.0 all-reduce.3.cloned.1.call-update
  41.6 0.0 all-gather.4.cloned.1.call-start
  41.6 0.5 all-gather.4.cloned.1.call-update
  42.1 1.3 copy.13
  43.5 6.3 %all-to-all-start = ((bf16[128,4,1024]{0,2,1:T(8,128)(2,1)}), bf16[128,4,1024]{0,2,1:T(8,128)(2,1)S(1)}, u32[]{:S(2)}, u32[]{:S(2)}) async-start(bf16[128,4,1024]{0,2,1:T(8,128)(2,1)} %bitcast), calls=%async_computation | async-start | bytes 2097152 | tf_op jit(solution)/shard_map/all_to_all | solution.py:31
  49.8 0.0 all-gather.6.cloned.1.call-start
  49.8 0.6 all-gather.6.cloned.1.call-update
  50.4 1.3 copy.15
  51.7 46.7 %all-to-all-done = bf16[128,4,1024]{0,2,1:T(8,128)(2,1)S(1)} async-done(((bf16[128,4,1024]{0,2,1:T(8,128)(2,1)}), bf16[128,4,1024]{0,2,1:T(8,128)(2,1)S(1)}, u32[]{:S(2)}, u32[]{:S(2)}) %all-to-all-start) | async-done | bytes 1048608 | tf_op jit(solution)/shard_map/all_to_all | solution.py:31
  98.4 3.5 %all-to-all-start.1 = ((bf16[128,4,1024]{0,2,1:T(8,128)(2,1)}), bf16[128,4,1024]{0,2,1:T(8,128)(2,1)S(1)}, u32[]{:S(2)}, u32[]{:S(2)}) async-start(bf16[128,4,1024]{0,2,1:T(8,128)(2,1)} %bitcast.5), calls=%async_computation.1 | async-start | bytes 2097152 | tf_op jit(solution)/shard_map/all_to_all | solution.py:32
  101.9 0.0 all-gather.8.cloned.1.call-start
  102.0 0.5 all-gather.8.cloned.1.call-update
  102.5 0.5 copy.14
  103.1 42.2 %all-to-all-done.1 = bf16[128,4,1024]{0,2,1:T(8,128)(2,1)S(1)} async-done(((bf16[128,4,1024]{0,2,1:T(8,128)(2,1)}), bf16[128,4,1024]{0,2,1:T(8,128)(2,1)S(1)}, u32[]{:S(2)}, u32[]{:S(2)}) %all-to-all-start.1) | async-done | bytes 1048608 | tf_op jit(solution)/shard_map/all_to_all | solution.py:32
  145.2 0.5 copy.16
  145.8 0.0 all-reduce.3.cloned.1.call-done
  145.8 41.5 %all-reduce.4 = bf16[128,4096]{1,0:T(8,128)(2,1)} all-reduce(f32[128,4096]{1,0:T(8,128)} %all-reduce.3.cloned.1.call-done), channel_id=1, replica_groups=mesh['rep'=4,'fs'=2,'tp'=4] {'tp'}, use_global_device_ids=true, to_apply=%region_1.0 | all-reduce | flops 524288 | bytes 3145728 | tf_op jit(solution)/shard_map/psum | solution.py:41
  187.3 5.6 %convolution_bitcast_fusion.1 = f32[1024,1408]{0,1:T(8,128)} fusion(bf16[512,1408]{1,0:T(8,128)(2,1)} %all-gather.4.cloned.1.call-done, bf16[512,1024]{1,0:T(8,128)(2,1)S(1)} %bitcast.29), kind=kOutput, calls=%fused_computation.2 | convolution fusion | flops 1476395008 | bytes 8257536 | tf_op jit(solution)/shard_map/dot_general | solution.py:8
  192.9 6.2 %copy.17 = f32[1024,1408]{1,0:T(8,128)} copy(f32[1024,1408]{0,1:T(8,128)} %convolution_bitcast_fusion.1) | data formatting | bytes 11534336
  199.1 5.6 %convolution_bitcast_fusion = f32[1024,1408]{0,1:T(8,128)} fusion(bf16[512,1408]{1,0:T(8,128)(2,1)} %all-gather.6.cloned.1.call-done, bf16[512,1024]{1,0:T(8,128)(2,1)S(1)} %bitcast.30), kind=kOutput, calls=%fused_computation.1 | convolution fusion | flops 1476395008 | bytes 8257536 | tf_op jit(solution)/shard_map/dot_general | solution.py:8
  204.7 6.2 %copy.18 = f32[1024,1408]{1,0:T(8,128)} copy(f32[1024,1408]{0,1:T(8,128)} %convolution_bitcast_fusion) | data formatting | bytes 11534336
  210.9 5.6 %fusion.4 = f32[1408,1024]{1,0:T(8,128)} fusion(bf16[512,1408]{1,0:T(8,128)(2,1)} %all-gather.8.cloned.1.call-done, bf16[512,1024]{1,0:T(8,128)(2,1)S(1)} %bitcast.28), kind=kOutput, calls=%fused_computation.11 | convolution fusion | flops 1476395008 | bytes 8257536 | tf_op jit(solution)/shard_map/dot_general | solution.py:8
  (9 shorter events, 0.0 us)
Async XLA Ops:
  8.0 8.6 %copy-start.2 = (bf16[128,4096]{1,0:T(8,128)(2,1)S(1)}, bf16[128,4096]{1,0:T(8,128)(2,1)}, u32[]{:S(2)}) copy-start(bf16[128,4096]{1,0:T(8,128)(2,1)} %param.5) | copy-start | bytes 3145732
  8.0 137.8 %all-reduce.3.cloned.1.call-start = ((), (), s32[]{:S(2)}) async-start(), calls=%async_computation.2 | async-start | bytes 4194304 | tf_op jit(solution)/shard_map/psum | solution.py:41
  8.1 8.6 %copy-start = (bf16[4096,1408]{1,0:T(8,128)(2,1)S(1)}, bf16[4096,1408]{1,0:T(8,128)(2,1)}, u32[]{:S(2)}) copy-start(bf16[4096,1408]{1,0:T(8,128)(2,1)} %param.7) | copy-start | bytes 34603012
  16.7 4.3 %copy-start.1 = (bf16[4096,1408]{1,0:T(8,128)(2,1)S(1)}, bf16[4096,1408]{1,0:T(8,128)(2,1)}, u32[]{:S(2)}) copy-start(bf16[4096,1408]{1,0:T(8,128)(2,1)} %param.8) | copy-start | bytes 34603012
  23.8 8.2 %copy-start.4 = (bf16[128,1408]{1,0:T(8,128)(2,1)}, bf16[128,1408]{1,0:T(8,128)(2,1)S(1)}, u32[]{:S(2)}) copy-start(bf16[128,1408]{1,0:T(8,128)(2,1)S(1)} %get-tuple-element.17) | copy-start | bytes 1081348
  41.5 8.8 %copy-start.3 = (bf16[128,4096]{1,0:T(8,128)(2,1)S(1)}, bf16[128,4096]{1,0:T(8,128)(2,1)}, u32[]{:S(2)}) copy-start(bf16[128,4096]{1,0:T(8,128)(2,1)} %param.6) | copy-start | bytes 3145732
  41.6 145.7 %all-gather.4.cloned.1.call-start = ((), (), s32[]{:S(2)}) async-start(), calls=%async_computation.3 | async-start | bytes 1802240 | tf_op jit(solution)/shard_map/all_gather | solution.py:34
  43.5 55.0 %all-to-all-start = ((bf16[128,4,1024]{0,2,1:T(8,128)(2,1)}), bf16[128,4,1024]{0,2,1:T(8,128)(2,1)S(1)}, u32[]{:S(2)}, u32[]{:S(2)}) async-start(bf16[128,4,1024]{0,2,1:T(8,128)(2,1)} %bitcast), calls=%async_computation | async-start | bytes 2097152 | tf_op jit(solution)/shard_map/all_to_all | solution.py:31
  49.8 149.3 %all-gather.6.cloned.1.call-start = ((), (), s32[]{:S(2)}) async-start(), calls=%async_computation.4 | async-start | bytes 1802240 | tf_op jit(solution)/shard_map/all_gather | solution.py:35
  98.4 46.8 %all-to-all-start.1 = ((bf16[128,4,1024]{0,2,1:T(8,128)(2,1)}), bf16[128,4,1024]{0,2,1:T(8,128)(2,1)S(1)}, u32[]{:S(2)}, u32[]{:S(2)}) async-start(bf16[128,4,1024]{0,2,1:T(8,128)(2,1)} %bitcast.5), calls=%async_computation.1 | async-start | bytes 2097152 | tf_op jit(solution)/shard_map/all_to_all | solution.py:32
  101.9 109.0 %all-gather.8.cloned.1.call-start = ((), (), s32[]{:S(2)}) async-start(), calls=%async_computation.5 | async-start | bytes 1802240 | tf_op jit(solution)/shard_map/all_gather | solution.py:36
Sparse Core Ops, SparseCore 0:
  41.7 65.6 all-reduce.2
Sparse Core Ops, SparseCore 1:
  44.2 54.8 all-gather.3
  100.5 46.3 all-gather.5
  148.3 33.7 all-gather.7
